TPU v7x, 32 devices: a whole 2x2x4 slice. The times are simulated.
32 devices in a mesh: ep: 4 (over y, x), tp: 8 (over z, core).
Axes of the slice: x: 2, y: 2, z: 4, core: 2. Of those that a mesh axis runs over, the one named last changes fastest.
Arguments:
- tokens: bfloat16 [64, 4096], P(None, 'ep'), may hold values from -60 to 60
- gain_attn: bfloat16 [4096], P('ep'), may hold values from 0.099609375 to 1.8984375
- w_query: bfloat16 [4096, 2048], P('ep', 'tp'), may hold values from -0.09375 to 0.09375
- w_key: bfloat16 [4096, 2048], P('ep', 'tp'), may hold values from -0.09375 to 0.09375
- w_value: bfloat16 [4096, 2048], P('ep', 'tp'), may hold values from -0.09375 to 0.09375
- w_output: bfloat16 [2048, 4096], P('tp', 'ep'), may hold values from -0.125 to 0.125
- key_cache: bfloat16 [64, 1024, 2048], P('ep', None, 'tp'), may hold values from -6 to 6
- value_cache: bfloat16 [64, 1024, 2048], P('ep', None, 'tp'), may hold values from -10 to 10
- lengths: int32 [64], P('ep'), may hold values from 128 to 1024
- score_shift: float32 [16], P('tp'), may hold values from -9.5 to -3.5
- gain_ffn: bfloat16 [4096], replicated, may hold values from 0.099609375 to 1.8984375
- w_mix: bfloat16 [4096], P('ep'), may hold values from -0.09375 to 0.09375
- w_dense_gate: bfloat16 [4096, 4096], P('ep', 'tp'), may hold values from -0.09375 to 0.09375
- w_dense_up: bfloat16 [4096, 4096], P('ep', 'tp'), may hold values from -0.09375 to 0.09375
- w_dense_down: bfloat16 [4096, 4096], P('tp', 'ep'), may hold values from -0.09375 to 0.09375
- route_group: int32 [64], replicated, may hold values from 0 to 3, as said below
- route_inner: int32 [64, 2], replicated, may hold values from 0 to 3, as said below
- route_weight: float32 [64, 2], replicated, may hold values from 0.3 to 1
- w_exp_gate: bfloat16 [16, 4096, 2048], P('ep', None, 'tp'), may hold values from -0.09375 to 0.09375
- w_exp_up: bfloat16 [16, 4096, 2048], P('ep', None, 'tp'), may hold values from -0.09375 to 0.09375
- w_exp_down: bfloat16 [16, 2048, 4096], P('ep', 'tp'), may hold values from -0.125 to 0.125
Outputs:
- mixed: bfloat16 [64, 4096], P(None, 'ep')
- new_keys: bfloat16 [64, 2048], P('ep', 'tp')
- new_values: bfloat16 [64, 2048], P('ep', 'tp')
Inputs may be any that keep to these rules, and one draw needn't show every extreme that they name: `route_group`: within every aligned block of 16 sequences (the sequences of one index of ep) exactly half of the tokens use one group, the same group in every block; the other groups share the rest. A token's 2 experts inside its group differ. Within every aligned block of 16 sequences no expert (route_group * 4 + route_inner) is used by more than 4 tokens, and the experts of the group that half of the block uses are each used by exactly 4.
All inputs are finite; a program needn't handle non-finite values.
Results may differ from a plain program's by a relative error of at most 0.0039.
The roundings to bfloat16 on the way count: a program that leaves them out, or rounds other values in their place, can miss the bound.
Values may be sent and summed in bfloat16 or wider, within the bound.
A program may use at most 128 MiB of HBM per device.

v0:
```python
import math

import jax
import jax.numpy as jnp
from jax import lax
from jax.sharding import PartitionSpec as P

D = 4096
HD = 128
EPG = 4
TOPK = 2
EXPERTS = 16
CAP = 4


norm_eps = 1e-06


def on_device(
    tokens,
    gain_attn,
    w_query,
    w_key,
    w_value,
    w_output,
    key_cache,
    value_cache,
    lengths,
    score_shift,
    gain_ffn,
    w_mix,
    w_dense_gate,
    w_dense_up,
    w_dense_down,
    route_group,
    route_inner,
    route_weight,
    w_exp_gate,
    w_exp_up,
    w_exp_down,
):
    ep_count = lax.axis_size("ep")
    batch_all, col_width = tokens.shape
    seq_local = batch_all // ep_count
    head_cols = w_query.shape[1]
    heads_local = head_cols // HD
    tokens_float = tokens.astype(jnp.float32)
    squares = lax.psum_scatter(
        jnp.sum(tokens_float * tokens_float, axis=1), "ep", scatter_dimension=0, tiled=True
    )
    inv_first = lax.rsqrt(squares / D + norm_eps)[:, None]
    scaled_in = (tokens_float * gain_attn.astype(jnp.float32)).astype(jnp.bfloat16)
    w_joint = jnp.concatenate([w_query, w_key, w_value], axis=1)
    joint_proj = (
        lax.psum_scatter(
            jnp.dot(scaled_in, w_joint, preferred_element_type=jnp.float32),
            "ep",
            scatter_dimension=0,
            tiled=True,
        )
        * inv_first
    )
    queries = joint_proj[:, :head_cols].astype(jnp.bfloat16)
    new_keys = joint_proj[:, head_cols : 2 * head_cols].astype(jnp.bfloat16)
    new_values = joint_proj[:, 2 * head_cols :].astype(jnp.bfloat16)
    cache_len = key_cache.shape[1]
    head_query = queries.reshape(seq_local, heads_local, HD)
    head_keys = key_cache.reshape(seq_local, cache_len, heads_local, HD)
    scores = jnp.einsum(
        "bhd,blhd->bhl", head_query, head_keys, preferred_element_type=jnp.float32
    ) / math.sqrt(HD)
    scores = scores + score_shift[None, :, None]
    live_mask = lax.broadcasted_iota(jnp.int32, scores.shape, 2) < lengths[:, None, None]
    soft_terms = jnp.where(live_mask, jax.nn.softplus(scores), 0.0)
    later_sum = lax.cumsum(soft_terms, axis=2, reverse=True) - soft_terms
    stick = jnp.where(live_mask, jnp.exp(jax.nn.log_sigmoid(scores) - later_sum), 0.0).astype(
        jnp.bfloat16
    )
    head_values = value_cache.reshape(seq_local, cache_len, heads_local, HD)
    attended = jnp.einsum("bhl,blhd->bhd", stick, head_values, preferred_element_type=jnp.float32)
    attended = attended.reshape(seq_local, head_cols).astype(jnp.bfloat16)
    attn_part = jnp.dot(
        lax.all_gather(attended, "ep", axis=0, tiled=True),
        w_output,
        preferred_element_type=jnp.float32,
    )
    attn_out = lax.psum(attn_part, "tp")
    middle = (tokens_float + attn_out).astype(jnp.bfloat16)
    middle_float = middle.astype(jnp.float32)
    gain_float = gain_ffn.astype(jnp.float32)
    gain_cols = lax.dynamic_slice_in_dim(gain_float, lax.axis_index("ep") * col_width, col_width, 0)
    scaled_mid = (middle_float * gain_cols).astype(jnp.bfloat16)
    dense_pre, dense_lin, mix_pre, mid_squares = lax.psum(
        (
            jnp.dot(scaled_mid, w_dense_gate, preferred_element_type=jnp.float32),
            jnp.dot(scaled_mid, w_dense_up, preferred_element_type=jnp.float32),
            jnp.dot(scaled_mid, w_mix, preferred_element_type=jnp.float32),
            jnp.sum(middle_float * middle_float, axis=1),
        ),
        "ep",
    )
    inv_second = lax.rsqrt(mid_squares / D + norm_eps)[:, None]
    dense_hidden = (jax.nn.silu(dense_pre * inv_second) * (dense_lin * inv_second)).astype(
        jnp.bfloat16
    )
    mix_gate = jax.nn.sigmoid(mix_pre * inv_second[:, 0])
    dense_part = (
        jnp.dot(dense_hidden, w_dense_down, preferred_element_type=jnp.float32) * mix_gate[:, None]
    )
    slot_count = CAP * ep_count
    expert_ids = (route_group[:, None] * EPG + route_inner).reshape(-1)
    expert_onehot = (expert_ids[:, None] == jnp.arange(EXPERTS, dtype=jnp.int32)[None, :]).astype(
        jnp.int32
    )
    per_block = expert_onehot.reshape(ep_count, seq_local * TOPK, EXPERTS)
    earlier = (jnp.cumsum(per_block, axis=1) - per_block).reshape(-1, EXPERTS)
    slot_rank = jnp.sum(earlier * expert_onehot, axis=1)
    route_index = jnp.arange(batch_all * TOPK, dtype=jnp.int32)
    block_of = route_index // (seq_local * TOPK)
    slot_flat = expert_ids * slot_count + block_of * CAP + slot_rank
    slot_table = (
        jnp.full((EXPERTS * slot_count,), batch_all, jnp.int32)
        .at[slot_flat]
        .set(route_index // TOPK)
    )
    padded_middle = jnp.concatenate([middle, jnp.zeros((1, col_width), jnp.bfloat16)], axis=0)
    outgoing = jnp.take(padded_middle, slot_table, axis=0).reshape(EXPERTS, slot_count, col_width)
    arrived_float = lax.all_to_all(outgoing, "ep", split_axis=0, concat_axis=2, tiled=True).astype(
        jnp.float32
    )
    inv_rows = lax.rsqrt(jnp.mean(arrived_float * arrived_float, axis=2, keepdims=True) + norm_eps)
    scaled_rows = (arrived_float * gain_float).astype(jnp.bfloat16)
    gate_pre = (
        jnp.einsum("end,edf->enf", scaled_rows, w_exp_gate, preferred_element_type=jnp.float32)
        * inv_rows
    )
    up_proj = (
        jnp.einsum("end,edf->enf", scaled_rows, w_exp_up, preferred_element_type=jnp.float32)
        * inv_rows
    )
    hidden = (jax.nn.silu(gate_pre) * up_proj).astype(jnp.bfloat16)
    expert_rows = jnp.einsum("enf,efd->end", hidden, w_exp_down, preferred_element_type=jnp.float32)
    returned = lax.all_to_all(expert_rows, "ep", split_axis=2, concat_axis=0, tiled=True)
    flat_back = returned.reshape(EXPERTS * slot_count, col_width)
    routed = jnp.take(flat_back, slot_flat, axis=0).reshape(batch_all, TOPK, col_width)
    expert_part = jnp.sum(routed * route_weight[:, :, None], axis=1)
    result_sum = middle_float + lax.psum(expert_part + dense_part, "tp")
    return (result_sum.astype(jnp.bfloat16), new_keys, new_values)


def solution(mesh):
    placed = (
        P(None, "ep"),
        P("ep"),
        P("ep", "tp"),
        P("ep", "tp"),
        P("ep", "tp"),
        P("tp", "ep"),
        P("ep", None, "tp"),
        P("ep", None, "tp"),
        P("ep"),
        P("tp"),
        P(),
        P("ep"),
        P("ep", "tp"),
        P("ep", "tp"),
        P("tp", "ep"),
        P(),
        P(),
        P(),
        P("ep", None, "tp"),
        P("ep", None, "tp"),
        P("ep", "tp", None),
    )
    return jax.shard_map(
        on_device,
        mesh=mesh,
        in_specs=placed,
        out_specs=(P(None, "ep"), P("ep", "tp"), P("ep", "tp")),
        check_vma=False,
    )
```

profile of v0, /device:TPU:0, one launch (start us, length us, event | category | flops | bytes accessed | tf_op | source)
XLA Modules:
  0.0 316.2 jit_solution(12506751394663622789)
XLA Ops:
  8.0 2.5 fusion.3
  10.6 1.0 fusion.14
  11.7 12.3 %copy.64 = bf16[16,1024,256]{1,2,0:T(8,128)(2,1)} copy(bf16[16,1024,256]{2,1,0:T(8,128)(2,1)} %param.27) | data formatting | bytes 16777216 | tf_op jit(solution)/shard_map/reshape | solution.py:68
  26.2 1.0 scatter_custom_fusion
  27.2 11.5 %all-reduce.1 = f32[64]{0:T(128)S(1)} all-reduce(f32[64]{0:T(128)S(1)} %fusion.14), channel_id=3, replica_groups=mesh['ep'=4,'tp'=8] {'ep'}, use_global_device_ids=true, to_apply=%region_2.0.clone | all-reduce | flops 64 | bytes 512
  40.3 4.6 %fusion.58 = f32[16,2,1,1024]{3,2,1,0:T(1,128)S(1)} fusion(bf16[16,2,128,1]{2,3,1,0:T(2,128)(2,1)S(1)} %reshape.226, bf16[16,1024,2,128]{1,3,2,0:T(8,128)(2,1)} %bitcast.59), kind=kOutput, calls=%fused_computation.104 | convolution fusion | flops 8388608 | bytes 8527872 | tf_op jit(solution)/shard_map/bhd,blhd->bhl/dot_general | solution.py:69
  45.4 39.6 %reduce-window.6 = f32[16,2,8,128]{3,2,1,0:T(8,128)S(1)} reduce-window(f32[16,2,8,128]{3,2,1,0:T(8,128)S(1)} %reshape.188, f32[]{:T(128)} %constant.94.clone.1), window={size=1x1x1x128 pad=0_0x0_0x0_0x0_127}, to_apply=%region_3.4 | reduce-window | flops 4161536 | bytes 262148 | tf_op jit(solution)/shard_map/reduce-window
  86.4 4.6 %fusion = f32[16,2,1,128]{3,2,1,0:T(1,128)S(1)} fusion(bf16[16,2,1024,1]{2,1,0,3:T(2,128)(2,1)S(1)} %fusion.42, bf16[16,1024,256]{2,1,0:T(8,128)(2,1)} %param.28), kind=kOutput, calls=%fused_computation.3 | convolution fusion | flops 8388608 | bytes 8470528 | tf_op jit(solution)/shard_map/bhl,blhd->bhd/dot_general | solution.py:80
  91.0 7.1 %all_gather.3 = bf16[64,256]{1,0:T(8,128)(2,1)S(1)} all-gather(bf16[16,256]{1,0:T(8,128)(2,1)S(1)} %bitcast.70), channel_id=1, replica_groups=mesh['ep'=4,'tp'=8] {'ep'}, dimensions={0}, use_global_device_ids=true | all-gather | bytes 40960 | tf_op jit(solution)/shard_map/all_gather | solution.py:83
  98.1 0.9 fusion.59
  99.2 55.8 %all-reduce.8.cloned.1.call-done = f32[64,1024]{1,0:T(8,128)} async-done(((f32[64,1024]{1,0:T(8,128)}), f32[64,1024]{1,0:T(8,128)}) %all-reduce.8.cloned.1.call-update) | async-done | bytes 262160 | tf_op jit(solution)/shard_map/psum | solution.py:87
  154.9 1.1 fusion.17
  156.0 1.2 gather_fusion
  158.1 3.6 %all-to-all-start = ((bf16[16,16,1024]{2,1,0:T(8,128)(2,1)}), bf16[16,16,1024]{2,1,0:T(8,128)(2,1)S(1)}, u32[]{:S(2)}, u32[]{:S(2)}) async-start(bf16[16,16,1024]{2,1,0:T(8,128)(2,1)} %broadcast_select_fusion), calls=%async_computation.1 | async-start | bytes 1048576 | tf_op jit(solution)/shard_map/all_to_all | solution.py:128
  162.3 6.1 %all-to-all-done = bf16[16,16,1024]{2,1,0:T(8,128)(2,1)S(1)} async-done(((bf16[16,16,1024]{2,1,0:T(8,128)(2,1)}), bf16[16,16,1024]{2,1,0:T(8,128)(2,1)S(1)}, u32[]{:S(2)}, u32[]{:S(2)}) %all-to-all-start) | async-done | bytes 524320 | tf_op jit(solution)/shard_map/all_to_all | solution.py:128
  168.4 1.5 copy.82
  169.8 1.9 reshape.192
  172.0 4.5 %convolution_multiply_fusion.2 = f32[4,16,256]{2,1,0:T(8,128)S(1)} fusion(bf16[4,4096,256]{2,1,0:T(8,128)(2,1)} %param.39, f32[4,16,4096]{2,1,0:T(8,128)S(1)} %reshape.192, f32[4096]{0:T(1024)S(1)} %convert_element_type.81, f32[4,16]{1,0:T(4,128)S(1)} %add_rsqrt_fusion), kind=kOutput, calls=%fused_computation.16 | convolution fusion | flops 134758400 | bytes 9519360 | tf_op jit(solution)/shard_map/end,edf->enf/dot_general | solution.py:134
  176.5 8.1 %fusion.12 = f32[4,16,4096]{2,1,0:T(8,128)S(1)} fusion(bf16[4,256,4096]{2,1,0:T(8,128)(2,1)} %param.41, bf16[4,4096,256]{2,1,0:T(8,128)(2,1)} %param.40, f32[4,16,4096]{2,1,0:T(8,128)S(1)} %reshape.192, f32[4096]{0:T(1024)S(1)} %convert_element_type.81, f32[4,16,256]{2,1,0:T(8,128)S(1)} %convolution_multiply_fusion.2, f32[4,16]{1,0:T(4,128)S(1)} %add_rsqrt_fusion), kind=kOutput, calls=%fused_computation.22 | convolution fusion | flops 269074432 | bytes 18956544 | tf_op jit(solution)/shard_map/enf,efd->end/dot_general | solution.py:142
  184.6 5.9 %copy.55 = f32[4,16,4096]{1,0,2:T(4,128)} copy(f32[4,16,4096]{2,1,0:T(8,128)S(1)} %fusion.12) | data formatting | bytes 2097152 | tf_op jit(solution)/shard_map/enf,efd->end/dot_general | solution.py:142
  190.5 8.8 %reshape.230 = f32[4,1,65536]{2,1,0:T(1,128)} reshape(f32[4096,4,16]{2,1,0:T(4,128)} %bitcast.60) | data formatting | bytes 2097152
  199.3 3.5 %all-to-all-start.1 = ((f32[4,1,65536]{2,1,0:T(1,128)}), f32[4,1,65536]{2,1,0:T(1,128)S(1)}, u32[]{:S(2)}, u32[]{:S(2)}) async-start(f32[4,1,65536]{2,1,0:T(1,128)} %reshape.230), calls=%async_computation.2 | async-start | bytes 2097152 | tf_op jit(solution)/shard_map/all_to_all | solution.py:143
  202.9 0.9 fusion.30
  203.8 2.2 fusion.32
  206.2 10.6 %all-reduce.2 = (f32[64]{0:T(128)S(1)}, f32[64]{0:T(128)S(1)}) all-reduce(f32[64]{0:T(128)S(1)} %convolution_bitcast_fusion, f32[64]{0:T(128)S(1)} %get-tuple-element.7), channel_id=1, replica_groups=mesh['ep'=4,'tp'=8] {'ep'}, use_global_device_ids=true, to_apply=%region_16.17 | all-reduce | flops 128 | bytes 1024 | tf_op jit(solution)/shard_map/psum | solution.py:93
  217.5 3.7 %reduce.5 = f32[4,65536]{1,0:T(4,128)S(1)} reduce(f32[4,1,65536]{2,1,0:T(1,128)S(1)} %all-to-all-done.1, f32[]{:T(128)} %broadcast.214), dimensions={1}, to_apply=%all_to_all.9.reduce_sub_computation | reduce | bytes 2097156 | tf_op jit(solution)/shard_map/all_to_all | solution.py:143
  221.2 9.1 %reshape.231 = f32[4096,4,16]{2,1,0:T(4,128)} reshape(f32[4,65536]{1,0:T(4,128)S(1)} %reduce.5) | data formatting | bytes 2097152
  230.3 6.7 %copy.56 = f32[4,16,4,1024]{3,1,0,2:T(8,128)S(1)} copy(f32[4,16,4,1024]{1,0,3,2:T(4,128)} %bitcast.61) | data formatting | bytes 2097152 | tf_op jit(solution)/shard_map/all_to_all | solution.py:143
  238.9 11.5 %all-reduce.12.cloned.1.call-done = (f32[64,512]{1,0:T(8,128)}, f32[64,512]{1,0:T(8,128)}) async-done(((f32[64,512]{1,0:T(8,128)}, f32[64,512]{1,0:T(8,128)}), (f32[64,512]{1,0:T(8,128)}, f32[64,512]{1,0:T(8,128)})) %all-reduce.12.cloned.1.call-update) | async-done | bytes 262160 | tf_op jit(solution)/shard_map/psum | solution.py:93
  250.4 2.0 fusion.9
  252.5 55.6 %all-reduce.10.cloned.1.call-done = f32[64,1024]{1,0:T(8,128)} async-done(((f32[64,1024]{1,0:T(8,128)}), f32[64,1024]{1,0:T(8,128)}) %all-reduce.10.cloned.1.call-update) | async-done | bytes 262160 | tf_op jit(solution)/shard_map/psum | solution.py:147
  308.1 1.6 fusion.18
  (87 shorter events, 10.3 us)
Async XLA Ops:
  7.2 243.3 %copy-start = (bf16[512,1024]{1,0:T(8,128)(2,1)S(1)}, bf16[512,1024]{1,0:T(8,128)(2,1)}, u32[]{:S(2)}) copy-start(bf16[512,1024]{1,0:T(8,128)(2,1)} %param.35) | copy-start | bytes 3145732
  7.2 31.6 %reduce-scatter.2.cloned.1.call-start = ((), (), s32[]{:S(2)}) async-start(), calls=%async_computation.3 | async-start | bytes 245760 | tf_op jit(solution)/shard_map/reduce_scatter | solution.py:55
  10.5 144.4 %all-reduce.8.cloned.1.call-start = ((), (), s32[]{:S(2)}) async-start(), calls=%async_computation.4 | async-start | bytes 524288 | tf_op jit(solution)/shard_map/psum | solution.py:87
  11.6 12.3 %copy-start.10 = (s32[64]{0:T(128)S(1)}, s32[64]{0:T(128)}, u32[]{:S(2)}) copy-start(s32[64]{0:T(128)} %param.36) | copy-start | bytes 772
  11.6 12.3 %copy-start.8 = (s32[64,2]{0,1:T(2,128)S(1)}, s32[64,2]{0,1:T(2,128)}, u32[]{:S(2)}) copy-start(s32[64,2]{0,1:T(2,128)} %param.37) | copy-start | bytes 1540
  11.6 13.3 %copy-start.11 = (u32[32]{0:T(128)S(1)}, u32[32]{0:T(128)}, u32[]{:S(2)}) copy-start(u32[32]{0:T(128)} %constant.122) | copy-start | bytes 388
  24.0 20.9 %copy-start.5 = (s32[16]{0:T(128)S(1)}, s32[16]{0:T(128)}, u32[]{:S(2)}) copy-start(s32[16]{0:T(128)} %param.29) | copy-start | bytes 196
  24.0 20.9 %copy-start.6 = (f32[2]{0:T(128)S(1)}, f32[2]{0:T(128)}, u32[]{:S(2)}) copy-start(f32[2]{0:T(128)} %param.30) | copy-start | bytes 28
  44.9 53.3 %copy-start.3 = (bf16[256,1024]{1,0:T(8,128)(2,1)S(1)}, bf16[256,1024]{1,0:T(8,128)(2,1)}, u32[]{:S(2)}) copy-start(bf16[256,1024]{1,0:T(8,128)(2,1)} %param.26) | copy-start | bytes 1572868
  44.9 110.1 %copy-start.2 = (bf16[64,1024]{1,0:T(8,128)(2,1)S(1)}, bf16[64,1024]{1,0:T(8,128)(2,1)}, u32[]{:S(2)}) copy-start(bf16[64,1024]{1,0:T(8,128)(2,1)} %param.21) | copy-start | bytes 393220
  86.3 75.5 %copy-start.4 = (bf16[4096]{0:T(1024)(128)(2,1)S(1)}, bf16[4096]{0:T(1024)(128)(2,1)}, u32[]{:S(2)}) copy-start(bf16[4096]{0:T(1024)(128)(2,1)} %param.31) | copy-start | bytes 24580
  86.4 75.8 %copy-start.9 = (f32[64,2]{0,1:T(2,128)S(1)}, f32[64,2]{0,1:T(2,128)}, u32[]{:S(2)}) copy-start(f32[64,2]{0,1:T(2,128)} %param.38) | copy-start | bytes 1540
  86.4 75.8 %copy-start.7 = (bf16[1024]{0:T(1024)(128)(2,1)S(1)}, bf16[1024]{0:T(1024)(128)(2,1)}, u32[]{:S(2)}) copy-start(bf16[1024]{0:T(1024)(128)(2,1)} %param.32) | copy-start | bytes 6148
  158.1 10.3 %all-to-all-start = ((bf16[16,16,1024]{2,1,0:T(8,128)(2,1)}), bf16[16,16,1024]{2,1,0:T(8,128)(2,1)S(1)}, u32[]{:S(2)}, u32[]{:S(2)}) async-start(bf16[16,16,1024]{2,1,0:T(8,128)(2,1)} %broadcast_select_fusion), calls=%async_computation.1 | async-start | bytes 1048576 | tf_op jit(solution)/shard_map/all_to_all | solution.py:128
  184.6 18.2 %copy-start.1 = (bf16[1024,512]{1,0:T(8,128)(2,1)S(1)}, bf16[1024,512]{1,0:T(8,128)(2,1)}, u32[]{:S(2)}) copy-start(bf16[1024,512]{1,0:T(8,128)(2,1)} %param.34) | copy-start | bytes 3145732
  199.3 17.6 %all-to-all-start.1 = ((f32[4,1,65536]{2,1,0:T(1,128)}), f32[4,1,65536]{2,1,0:T(1,128)S(1)}, u32[]{:S(2)}, u32[]{:S(2)}) async-start(f32[4,1,65536]{2,1,0:T(1,128)} %reshape.230), calls=%async_computation.2 | async-start | bytes 2097152 | tf_op jit(solution)/shard_map/all_to_all | solution.py:143
  202.8 47.6 %all-reduce.12.cloned.1.call-start = ((), (), s32[]{:S(2)}) async-start(), calls=%async_computation.6 | async-start | bytes 524288 | tf_op jit(solution)/shard_map/psum | solution.py:93
  206.0 102.0 %all-reduce.10.cloned.1.call-start = ((), (), s32[]{:S(2)}) async-start(), calls=%async_computation.5 | async-start | bytes 524288 | tf_op jit(solution)/shard_map/psum | solution.py:147
Sparse Core Ops, SparseCore 0:
  10.7 26.9 reduce-scatter.1
  99.2 55.6 all-reduce.7
  207.1 43.2 all-reduce.11
  252.6 55.4 all-reduce.9
where the time goes:
time: 317 us; the launch traced here: 316 us
  waiting for transfers between devices  129 us (41%)
  local copies, waits for them, and re-layouts  52.7 us (17%)
  other arithmetic  52.6 us (17%)
  matrix products  30.5 us (10%)
  blocking collectives  29.3 us (9%)
  between operations  14.8 us (5%)
  starting transfers between devices  7.33 us (2%)
    psum x1, waiting for transfers between devices, on_device(): attn_out = lax.psum(attn_part, 'tp')  55.8 us
    psum x1, waiting for transfers between devices, on_device(): result_sum = middle_float + lax.psum(expert_part + dense_part, 'tp')  55.6 us
    another operation x3, other arithmetic  40.5 us
    unnamed x30, local copies, waits for them, and re-layouts  18.6 us
    reshape x1, local copies, waits for them, and re-layouts, on_device(): head_keys = key_cache.reshape(seq_local, cache_len, heads_local, HD)  12.3 us
    psum x1, waiting for transfers between devices, on_device(): lax.psum((jnp.dot(scaled_mid, w_dense_gate, preferred_element_type=jnp.fl...  11.5 us
    unnamed x1, blocking collectives  11.5 us
    psum x1, blocking collectives, on_device(): lax.psum((jnp.dot(scaled_mid, w_dense_gate, preferred_element_type=jnp.fl...  10.6 us
  transfers between devices with their start and end apart: 6, of which 4 were waited for; matrix products, arithmetic and copies ran while one was open for 13% of the time, Pallas kernels for 0%

commit v1 on v0

v1 whole, which is shorter than its diff:
```python
import functools
import math

import jax
import jax.numpy as jnp
from jax import lax
from jax.experimental import pallas as pl
from jax.experimental.pallas import tpu as pltpu
from jax.sharding import PartitionSpec as P

HD = 128
EPG = 4
LANES = 128
MESH = pl.DeviceIdType.MESH
BF = jnp.bfloat16
F32 = jnp.float32

norm_eps = 1e-06


def dot(a, b):
    return jnp.dot(a, b, preferred_element_type=F32)


def silu(v):
    return v / (1.0 + jnp.exp(-v))


def sigmoid(v):
    return 1.0 / (1.0 + jnp.exp(-v))


def layer_kernel(
    n_ep,
    n_tp,
    tok_ref, gain_a_ref, mix_ref, gain_f_ref, len_ref, shift_ref, ids_ref, rw_ref,
    wq_h, wk_h, wv_h, kc_h, vc_h, wo_h, wdg_h, wdu_h, weg_h, weu_h, wed_h, wdd_h,
    mixed_ref, nk_ref, nv_ref,
    wqkv, kc, vc, wo, wdg, wdu, weg, weu, wed, wdd,
    qkv_s, qkv_r, mix_all, att_all, out_s, out_r, mid_own, mid_all, x_own, x_all,
    den_s, den_r, hid_own, hid_all, exp_s, exp_r, fin_s, fin_r, row_own, row_all,
    tok_f, score, att, part, xs, acc_g, acc_u, hid, total,
    w_sem, ep_ss, ep_rs, tp_ss, tp_rs,
):
    ep, tp = lax.axis_index("ep"), lax.axis_index("tp")
    batch, cols = tok_ref.shape
    seqs = batch // n_ep
    rows = batch // n_tp
    width = wq_h.shape[1]
    heads = width // HD
    length = kc.shape[1]
    ff = wdg.shape[1]
    local_experts = weg.shape[0]
    d_model = weg.shape[1]

    loads = {}

    def load(name, src, dst, k):
        loads[name] = pltpu.make_async_copy(src, dst, w_sem.at[k])
        loads[name].start()

    load("q", wq_h, wqkv.at[:, pl.ds(0, width)], 0)
    load("k", wk_h, wqkv.at[:, pl.ds(width, width)], 1)
    load("v", wv_h, wqkv.at[:, pl.ds(2 * width, width)], 2)
    load("kc", kc_h, kc, 3)
    load("vc", vc_h, vc, 4)
    load("wo", wo_h, wo, 5)
    load("wdg", wdg_h, wdg, 6)
    load("wdu", wdu_h, wdu, 7)
    load("weg", weg_h, weg, 8)
    load("weu", weu_h, weu, 9)
    load("wed", wed_h, wed, 10)
    load("wdd", wdd_h, wdd, 11)

    barrier = pltpu.get_barrier_semaphore()
    for d in range(1, n_ep):
        pl.semaphore_signal(
            barrier, inc=1, device_id={"ep": lax.rem(ep + d, n_ep)}, device_id_type=MESH
        )
    for d in range(1, n_tp):
        pl.semaphore_signal(
            barrier, inc=1, device_id={"tp": lax.rem(tp + d, n_tp)}, device_id_type=MESH
        )

    def send(axis, stage, src, dst):
        me, n, ss, rs = (ep, n_ep, ep_ss, ep_rs) if axis == "ep" else (tp, n_tp, tp_ss, tp_rs)
        copies = []
        for d in range(1, n):
            peer = lax.rem(me + d, n)
            copy = pltpu.make_async_remote_copy(
                src_ref=src(peer, d),
                dst_ref=dst(me, d),
                send_sem=ss.at[stage, d],
                recv_sem=rs.at[stage, d],
                device_id={axis: peer},
                device_id_type=MESH,
            )
            copy.start()
            copies.append(copy)
        return copies

    def finish(copies):
        for copy in copies:
            copy.wait()

    tokens = tok_ref[...].astype(F32)
    tok_f[...] = tokens
    scaled_in = (tokens * gain_a_ref[...].astype(F32)).astype(BF)
    for name in ("q", "k", "v"):
        loads[name].wait()
    qkv_s[:, : 3 * width] = dot(scaled_in, wqkv[...])
    qkv_s[:, 3 * width :] = jnp.broadcast_to(
        jnp.sum(tokens * tokens, axis=1, keepdims=True), (batch, LANES)
    )
    pl.semaphore_wait(barrier, n_ep + n_tp - 2)
    copies = send(
        "ep", 0, lambda peer, d: qkv_s.at[pl.ds(peer * seqs, seqs)], lambda me, d: qkv_r.at[d]
    )
    mix_copies = send("ep", 1, lambda peer, d: mix_ref, lambda me, d: mix_all.at[d])
    joint = qkv_s[pl.ds(ep * seqs, seqs), :]
    finish(copies)
    for d in range(1, n_ep):
        joint = joint + qkv_r[d]
    inv_first = lax.rsqrt(joint[:, 3 * width : 3 * width + 1] / d_model + norm_eps)
    joint = joint[:, : 3 * width] * inv_first
    queries = joint[:, :width].astype(BF).astype(F32)
    nk_ref[...] = joint[:, width : 2 * width].astype(BF)
    nv_ref[...] = joint[:, 2 * width :].astype(BF)

    lane_head = lax.broadcasted_iota(jnp.int32, (seqs, width), 1) // HD
    head_query = jnp.concatenate(
        [jnp.where(lane_head == h, queries, 0.0) for h in range(heads)], axis=0
    ).astype(BF)
    loads["kc"].wait()
    for s in range(seqs):
        found = lax.dot_general(
            head_query, kc[s], (((1,), (1,)), ((), ())), preferred_element_type=F32
        )
        for h in range(heads):
            score[h * seqs + s : h * seqs + s + 1, :] = found[h * seqs + s : h * seqs + s + 1, :]
    all_rows = heads * seqs
    scores = score[...] * (1.0 / math.sqrt(HD)) + shift_ref[...]
    live = lax.broadcasted_iota(jnp.int32, (all_rows, length), 1) < len_ref[...]
    tail = jnp.log1p(jnp.exp(-jnp.abs(scores)))
    soft = jnp.where(live, jnp.maximum(scores, 0.0) + tail, 0.0)
    chunks = length // LANES
    stacked = jnp.concatenate(
        [soft[:, c * LANES : (c + 1) * LANES] for c in range(chunks)], axis=0
    )
    later = (
        lax.broadcasted_iota(jnp.int32, (LANES, LANES), 0)
        > lax.broadcasted_iota(jnp.int32, (LANES, LANES), 1)
    ).astype(F32).astype(BF)
    high = stacked.astype(BF)
    rest = stacked - high.astype(F32)
    mid = rest.astype(BF)
    low = (rest - mid.astype(F32)).astype(BF)
    inner = dot(high, later) + (dot(mid, later) + dot(low, later))
    sums = jnp.sum(stacked, axis=1, keepdims=True)
    running = jnp.zeros((all_rows, 1), F32)
    pieces = [None] * chunks
    for c in reversed(range(chunks)):
        pieces[c] = inner[c * all_rows : (c + 1) * all_rows] + running
        running = running + sums[c * all_rows : (c + 1) * all_rows]
    later_sum = jnp.concatenate(pieces, axis=1)
    stick = jnp.where(
        live, jnp.exp(jnp.minimum(scores, 0.0) - tail - later_sum), 0.0
    ).astype(BF)
    loads["vc"].wait()
    for s in range(seqs):
        found = dot(stick, vc[s])
        for h in range(heads):
            att[s : s + 1, h * HD : (h + 1) * HD] = found[
                h * seqs + s : h * seqs + s + 1, h * HD : (h + 1) * HD
            ]
    att_all[ep] = att[...].astype(BF)
    copies = send("ep", 2, lambda peer, d: att_all.at[ep], lambda me, d: att_all.at[me])
    finish(mix_copies)
    loads["wo"].wait()
    finish(copies)

    part[...] = dot(att_all[...].reshape(batch, width), wo[...])
    for t in range(n_tp):
        out_s[t] = part[t * rows : (t + 1) * rows, :].astype(BF)
    copies = send("tp", 0, lambda peer, d: out_s.at[peer], lambda me, d: out_r.at[d])
    my_rows = pl.ds(pl.multiple_of(tp * rows, rows), rows)
    attn_out = part[my_rows, :]
    finish(copies)
    for d in range(1, n_tp):
        attn_out = attn_out + out_r[d].astype(F32)
    mid_own[...] = (tok_f[my_rows, :] + attn_out).astype(BF)
    mid_all[tp] = mid_own[...]
    copies = send("tp", 1, lambda peer, d: mid_own, lambda me, d: mid_all.at[me])
    finish(copies)
    middle = jnp.concatenate([mid_all[t].astype(F32) for t in range(n_tp)], axis=0)
    x_own[...] = middle.astype(BF)
    x_copies = send("ep", 3, lambda peer, d: x_own, lambda me, d: x_all.at[d])

    def features(d, block, squares, mixing):
        owner = lax.rem(ep - d + n_ep, n_ep)
        at = pl.ds(pl.multiple_of(owner * cols, cols), cols)
        scaled = (block * gain_f_ref[:, at].astype(F32)).astype(BF)
        xs[d] = scaled
        mix_row = mix_ref[0:1, :] if d == 0 else mix_all[d, 0:1, :]
        squares = squares + jnp.sum(block * block, axis=1, keepdims=True)
        mixing = mixing + jnp.sum(scaled.astype(F32) * mix_row, axis=1, keepdims=True)
        return at, squares, mixing

    def experts(d, at):
        def one(e, carry):
            gate = dot(xs[d], weg[e, at, :])
            up = dot(xs[d], weu[e, at, :])
            if d == 0:
                acc_g[e] = gate
                acc_u[e] = up
            else:
                acc_g[e] = acc_g[e] + gate
                acc_u[e] = acc_u[e] + up
            return carry

        lax.fori_loop(0, local_experts, one, 0)

    zero = jnp.zeros((batch, 1), F32)
    at, squares, mixing = features(0, middle, zero, zero)
    loads["wdg"].wait()
    loads["wdu"].wait()
    part[:, :ff] = dot(xs[0], wdg[...])
    total[:, :ff] = dot(xs[0], wdu[...])
    for e in range(n_ep):
        den_s[e, :, :ff] = part[e * seqs : (e + 1) * seqs, :ff].astype(BF)
        den_s[e, :, ff:] = total[e * seqs : (e + 1) * seqs, :ff].astype(BF)
    den_copies = send("ep", 4, lambda peer, d: den_s.at[peer], lambda me, d: den_r.at[d])
    my_seqs = pl.ds(pl.multiple_of(ep * seqs, seqs), seqs)
    dense_pre = part[my_seqs, :ff]
    dense_lin = total[my_seqs, :ff]
    loads["weg"].wait()
    loads["weu"].wait()
    experts(0, at)
    for d in range(1, n_ep):
        x_copies[d - 1].wait()
        at, squares, mixing = features(d, x_all[d].astype(F32), squares, mixing)
        experts(d, at)
    inv_second = lax.rsqrt(squares / d_model + norm_eps)
    mix_gate = sigmoid(mixing * inv_second)

    total[:, :LANES] = jnp.broadcast_to(inv_second, (batch, LANES))
    my_inv = total[my_seqs, :LANES][:, :1]
    finish(den_copies)
    for d in range(1, n_ep):
        dense_pre = dense_pre + den_r[d, :, :ff].astype(F32)
        dense_lin = dense_lin + den_r[d, :, ff:].astype(F32)
    hid_own[...] = (silu(dense_pre * my_inv) * (dense_lin * my_inv)).astype(BF)
    hid_all[ep] = hid_own[...]
    hid_copies = send("ep", 5, lambda peer, d: hid_own, lambda me, d: hid_all.at[me])

    for e in range(local_experts):
        hid[e] = (silu(acc_g[e] * inv_second) * (acc_u[e] * inv_second)).astype(BF)

    loads["wed"].wait()

    def down(owner):
        at = pl.ds(pl.multiple_of(owner * cols, cols), cols)
        total[...] = jnp.zeros_like(total)

        def one(e, carry):
            mine = ids_ref[...] == ep * local_experts + e
            weight = jnp.sum(jnp.where(mine, rw_ref[...], 0.0), axis=1, keepdims=True)
            total[...] += dot(hid[e], wed[e, :, at]) * weight
            return carry

        lax.fori_loop(0, local_experts, one, 0)

    exp_copies = []
    for d in range(1, n_ep):
        peer = lax.rem(ep + d, n_ep)
        down(peer)
        exp_s[d] = total[...].astype(BF)
        copy = pltpu.make_async_remote_copy(
            src_ref=exp_s.at[d],
            dst_ref=exp_r.at[d],
            send_sem=ep_ss.at[6, d],
            recv_sem=ep_rs.at[6, d],
            device_id={"ep": peer},
            device_id_type=MESH,
        )
        copy.start()
        exp_copies.append(copy)
    down(ep)
    loads["wdd"].wait()
    finish(hid_copies)
    total[...] += dot(hid_all[...].reshape(batch, ff), wdd[...]) * mix_gate
    for d in range(1, n_ep):
        exp_copies[d - 1].wait()
        total[...] += exp_r[d].astype(F32)

    for t in range(n_tp):
        fin_s[t] = total[t * rows : (t + 1) * rows, :].astype(BF)
    copies = send("tp", 2, lambda peer, d: fin_s.at[peer], lambda me, d: fin_r.at[d])
    result = total[my_rows, :] + mid_own[...].astype(F32)
    finish(copies)
    for d in range(1, n_tp):
        result = result + fin_r[d].astype(F32)
    row_own[...] = result.astype(BF)
    row_all[tp] = row_own[...]
    copies = send("tp", 3, lambda peer, d: row_own, lambda me, d: row_all.at[me])
    finish(copies)
    mixed_ref[...] = jnp.concatenate(
        [row_all[t].astype(F32) for t in range(n_tp)], axis=0
    ).astype(BF)


def on_device(
    n_ep,
    n_tp,
    tokens,
    gain_attn,
    w_query,
    w_key,
    w_value,
    w_output,
    key_cache,
    value_cache,
    lengths,
    score_shift,
    gain_ffn,
    w_mix,
    w_dense_gate,
    w_dense_up,
    w_dense_down,
    route_group,
    route_inner,
    route_weight,
    w_exp_gate,
    w_exp_up,
    w_exp_down,
):
    batch, cols = tokens.shape
    seqs, rows = batch // n_ep, batch // n_tp
    width = w_query.shape[1]
    heads = width // HD
    length = key_cache.shape[1]
    ff = w_dense_gate.shape[1]
    local_experts, d_model, unit = w_exp_gate.shape
    vm, hbm = pl.BlockSpec(memory_space=pltpu.VMEM), pl.BlockSpec(memory_space=pl.ANY)
    small = (
        tokens,
        gain_attn.reshape(1, cols),
        jnp.broadcast_to(w_mix.astype(F32)[None, :], (8, cols)),
        gain_ffn.reshape(1, d_model),
        jnp.tile(lengths, heads)[:, None],
        jnp.repeat(score_shift, seqs)[:, None],
        route_group[:, None] * EPG + route_inner,
        route_weight,
    )
    large = (
        w_query, w_key, w_value, key_cache, value_cache, w_output,
        w_dense_gate, w_dense_up, w_exp_gate, w_exp_up, w_exp_down, w_dense_down,
    )

    def buf(*shape, kind=BF):
        return pltpu.VMEM(shape, kind)

    scratch = [
        buf(cols, 3 * width),
        buf(*key_cache.shape),
        buf(*value_cache.shape),
        buf(*w_output.shape),
        buf(*w_dense_gate.shape),
        buf(*w_dense_up.shape),
        buf(*w_exp_gate.shape),
        buf(*w_exp_up.shape),
        buf(*w_exp_down.shape),
        buf(*w_dense_down.shape),
        buf(batch, 3 * width + LANES, kind=F32),
        buf(n_ep, seqs, 3 * width + LANES, kind=F32),
        buf(n_ep, 8, cols, kind=F32),
        buf(n_ep, seqs, width),
        buf(n_tp, rows, cols),
        buf(n_tp, rows, cols),
        buf(rows, cols),
        buf(n_tp, rows, cols),
        buf(batch, cols),
        buf(n_ep, batch, cols),
        buf(n_ep, seqs, 2 * ff),
        buf(n_ep, seqs, 2 * ff),
        buf(seqs, ff),
        buf(n_ep, seqs, ff),
        buf(n_ep, batch, cols),
        buf(n_ep, batch, cols),
        buf(n_tp, rows, cols),
        buf(n_tp, rows, cols),
        buf(rows, cols),
        buf(n_tp, rows, cols),
        buf(batch, cols, kind=F32),
        buf(heads * seqs, length, kind=F32),
        buf(seqs, width, kind=F32),
        buf(batch, cols, kind=F32),
        buf(n_ep, batch, cols),
        buf(local_experts, batch, unit, kind=F32),
        buf(local_experts, batch, unit, kind=F32),
        buf(local_experts, batch, unit),
        buf(batch, cols, kind=F32),
        pltpu.SemaphoreType.DMA((12,)),
        pltpu.SemaphoreType.DMA((7, n_ep)),
        pltpu.SemaphoreType.DMA((7, n_ep)),
        pltpu.SemaphoreType.DMA((4, n_tp)),
        pltpu.SemaphoreType.DMA((4, n_tp)),
    ]
    return pl.pallas_call(
        functools.partial(layer_kernel, n_ep, n_tp),
        out_shape=(
            jax.ShapeDtypeStruct((batch, cols), BF),
            jax.ShapeDtypeStruct((seqs, width), BF),
            jax.ShapeDtypeStruct((seqs, width), BF),
        ),
        in_specs=[vm] * len(small) + [hbm] * len(large),
        out_specs=(vm, vm, vm),
        scratch_shapes=scratch,
        compiler_params=pltpu.CompilerParams(
            collective_id=0, has_side_effects=True, vmem_limit_bytes=62 * 1024 * 1024
        ),
        name="layer",
    )(*small, *large)


def solution(mesh):
    placed = (
        P(None, "ep"),
        P("ep"),
        P("ep", "tp"),
        P("ep", "tp"),
        P("ep", "tp"),
        P("tp", "ep"),
        P("ep", None, "tp"),
        P("ep", None, "tp"),
        P("ep"),
        P("tp"),
        P(),
        P("ep"),
        P("ep", "tp"),
        P("ep", "tp"),
        P("tp", "ep"),
        P(),
        P(),
        P(),
        P("ep", None, "tp"),
        P("ep", None, "tp"),
        P("ep", "tp", None),
    )
    return jax.shard_map(
        functools.partial(on_device, mesh.shape["ep"], mesh.shape["tp"]),
        mesh=mesh,
        in_specs=placed,
        out_specs=(P(None, "ep"), P("ep", "tp"), P("ep", "tp")),
        check_vma=False,
    )
```

time: 317 us -> 71.7 us (0.23)
  waiting for transfers between devices: 129 us -> 0 us
  Pallas kernels: 0 us -> 56.3 us
  other arithmetic: 52.6 us -> 1.34 us
  local copies, waits for them, and re-layouts: 52.7 us -> 12.9 us
  matrix products: 30.5 us -> 0 us
  blocking collectives: 29.3 us -> 0 us
  between operations: 14.8 us -> 0.64 us
  starting transfers between devices: 7.33 us -> 0 us
    psum x3 -> x0, waiting for transfers between devices: 123 us -> none  [the longest x1 55.8 us: on_device(): attn_out = lax.psum(attn_part, 'tp')]
    pallas_call x0 -> x1, Pallas kernels: none -> 56.3 us  [on_device(): pl.pallas_call(functools.partial(layer_kernel, n_ep, n_tp), out_shape=(ja...]
    another operation x5 -> x0, other arithmetic: 40.7 us -> none
    dot_general x10 -> x0, matrix products: 30.5 us -> none  [the longest x1 8.1 us: on_device(): jnp.einsum('enf,efd->end', hidden, w_exp_down, preferred_element_type=jnp...]
    unnamed x30 -> x5, local copies, waits for them, and re-layouts: 18.6 us -> 6.31 us
    unnamed x1 -> x0, blocking collectives: 11.5 us -> none
    psum x1 -> x0, blocking collectives: 10.6 us -> none  [on_device(): lax.psum((jnp.dot(scaled_mid, w_dense_gate, preferred_element_type=jnp.fl...]
    reshape x3 -> x2, local copies, waits for them, and re-layouts: 12.4 us -> 2.58 us  [the longest x1 1.3 us: on_device(): gain_ffn.reshape(1, d_model)]
  transfers between devices with their start and end apart: 6 -> 0, of which waited for: 4 -> 0; matrix products, arithmetic and copies ran while one was open for 13% -> 0% of each run, Pallas kernels for 0% -> 0%
where the time goes in v1:
time: 71.7 us; the launch traced here: 71.2 us
  Pallas kernels  56.3 us (79%)
  local copies, waits for them, and re-layouts  12.9 us (18%)
  other arithmetic  1.34 us (2%)
    pallas_call x1, Pallas kernels, on_device(): pl.pallas_call(functools.partial(layer_kernel, n_ep, n_tp), out_shape=(ja...  56.3 us
    unnamed x5, local copies, waits for them, and re-layouts  6.31 us

profile of v1, /device:TPU:0, one launch (start us, length us, event | category | flops | bytes accessed | tf_op | source)
XLA Modules:
  0.0 71.2 jit_solution(14074273829030411932)
XLA Ops:
  0.6 0.7 broadcast_multiply_fusion
  1.3 0.7 tile.2
  1.9 0.7 %broadcast_in_dim.5 = f32[2,16]{1,0:T(2,128)S(1)} broadcast(f32[2]{0:T(128)} %param.30), dimensions={0} | broadcast | bytes 136 | tf_op jit(solution)/shard_map/broadcast_in_dim | solution.py:351
  2.7 1.3 %reshape.16.gain_a_ref = bf16[1,1024]{1,0:T(2,128)(2,1)} reshape(bf16[1024]{0:T(1024)(128)(2,1)} %param.22) | data formatting | bytes 4096 | tf_op jit(solution)/shard_map/reshape | solution.py:347
  3.9 0.7 broadcast_in_dim_reshape.4.shift_ref
  4.6 0.7 broadcast_in_dim_tile.4.len_ref
  5.3 1.3 %reshape.17.gain_f_ref = bf16[1,4096]{1,0:T(2,128)(2,1)} reshape(bf16[4096]{0:T(1024)(128)(2,1)} %param.31) | data formatting | bytes 16384 | tf_op jit(solution)/shard_map/reshape | solution.py:349
  6.6 1.3 %broadcast_in_dim.4.mix_ref = f32[8,1024]{1,0:T(8,128)} broadcast(bf16[1024]{0:T(1024)(128)(2,1)} %param.32), dimensions={1} | broadcast | bytes 34816 | tf_op jit(solution)/shard_map/broadcast_in_dim | solution.py:348
  7.9 0.8 %copy.29 = s32[64,2]{1,0:T(8,128)S(1)} copy(s32[64,2]{0,1:T(2,128)} %param.37) | data formatting | bytes 1024 | tf_op args[16]
  8.7 0.7 broadcast_add_fusion.ids_ref
  9.4 1.4 %copy.32.rw_ref = f32[64,2]{1,0:T(8,128)} copy(f32[64,2]{0,1:T(2,128)} %param.38) | data formatting | bytes 1024 | tf_op args[17]
  10.8 56.3 %layer.1 = (bf16[64,1024]{1,0:T(8,128)(2,1)}, bf16[16,256]{1,0:T(8,128)(2,1)}, bf16[16,256]{1,0:T(8,128)(2,1)}) custom-call(bf16[64,1024]{1,0:T(8,128)(2,1)} %tok_ref.1, bf16[1,1024]{1,0:T(2,128)(2,1)} %reshape.16.gain_a_ref, f32[8,1024]{1,0:T(8,128)} %broadcast_in_dim.4.mix_ref, bf16[1,4096]{1,0:T(2,128)(2,1)} %reshape.17.gain_f_ref, ...), custom_call_target="tpu_custom_call" | custom-call | tf_op jit(solution)/shard_map/layer/pallas_call | solution.py:409
  67.1 1.6 %copy.36 = bf16[64,1024]{1,0:T(8,128)(2,1)} copy(bf16[64,1024]{1,0:T(8,128)(2,1)} %get-tuple-element.6) | data formatting | bytes 262144
  68.6 1.3 %copy.37 = bf16[16,256]{1,0:T(8,128)(2,1)} copy(bf16[16,256]{1,0:T(8,128)(2,1)} %get-tuple-element.7) | data formatting | bytes 16384
  69.9 1.3 %copy.38 = bf16[16,256]{1,0:T(8,128)(2,1)} copy(bf16[16,256]{1,0:T(8,128)(2,1)} %get-tuple-element.8) | data formatting | bytes 16384
